TPU v7x, 32 devices: a whole 2x2x4 slice. The times are simulated.
32 devices in a mesh: ep: 8 (over z, x), tp: 4 (over y, core).
Axes of the slice: x: 2, y: 2, z: 4, core: 2. Of those that a mesh axis runs over, the one named last changes fastest.
Arguments:
- tokens: bfloat16 [256, 2048], P('ep'), may hold values from -6 to 6
- state: float32 [256, 16, 128, 128], P('ep', 'tp'), may hold values from -6 to 6
- norm_gain: float32 [2048], replicated, may hold values from 0.1 to 1.9
- w_query: bfloat16 [2048, 2048], P(None, 'tp'), may hold values from -0.125 to 0.125
- w_forget: bfloat16 [2048, 2048], P(None, 'tp'), may hold values from -0.125 to 0.125
- w_input: bfloat16 [2048, 2048], P(None, 'tp'), may hold values from -0.125 to 0.125
- w_outgate: bfloat16 [2048, 2048], P(None, 'tp'), may hold values from -0.125 to 0.125
- forget_floor: float32 [2048], P('tp'), may hold values from 0.05 to 0.95
- head_gain: float32 [128], replicated, may hold values from 0.1 to 1.9
- w_out: bfloat16 [2048, 2048], P('tp'), may hold values from -0.125 to 0.125
- ffn_gain: float32 [2048], replicated, may hold values from 0.1 to 1.9
- routes: int32 [256, 2], P('ep'), may hold values from 0 to 7, all different within a row; in each aligned block of 32 rows (0 to 31, 32 to 63, ...) at most 16 rows name the same one
- route_weights: float32 [256, 2], P('ep'), may hold values from 0.2 to 1
- expert_gate: bfloat16 [8, 2048, 5632], P('ep', None, 'tp'), may hold values from -0.125 to 0.125
- expert_up: bfloat16 [8, 2048, 5632], P('ep', None, 'tp'), may hold values from -0.125 to 0.125
- expert_down: bfloat16 [8, 5632, 2048], P('ep', 'tp'), may hold values from -0.078125 to 0.078125
- dense_gate: bfloat16 [2048, 5632], P(None, 'ep'), may hold values from -0.125 to 0.125
- dense_up: bfloat16 [2048, 5632], P(None, 'ep'), may hold values from -0.125 to 0.125
- dense_down: bfloat16 [5632, 2048], P('ep'), may hold values from -0.078125 to 0.078125
- dense_mix: float32 [2048], replicated, may hold values from -6 to 6
Outputs:
- mixed: bfloat16 [256, 2048], P('ep')
- new_state: float32 [256, 16, 128, 128], P('ep', 'tp')
Inputs may be any that keep to these rules, and one draw needn't show every extreme that they name: `routes`: each row names 2 different experts; the rows of one index of ep name no expert more than 16 times, a bound that some block reaches.
All inputs are finite; a program needn't handle non-finite values.
Results may differ from a plain program's by a relative error of at most 0.014.
Values may be sent and summed in bfloat16 or wider, within the bound.
A program may use at most 128 MiB of HBM per device.

v0:
```python
import jax
import jax.numpy as jnp
from jax import lax
from jax.sharding import PartitionSpec as P

EPS = 1e-06


def rms_norm(value, gain):
    return value * lax.rsqrt(jnp.mean(value * value, axis=-1, keepdims=True) + EPS) * gain


def make_table(local_routes, experts, capacity):
    flat = local_routes.reshape(-1)
    onehot = (flat[:, None] == jnp.arange(experts, dtype=jnp.int32)[None, :]).astype(jnp.int32)
    before = jnp.cumsum(onehot, axis=0) - onehot
    slot = jnp.sum(before * onehot, axis=1)
    where = flat * capacity + slot
    return (where[:, None] == jnp.arange(experts * capacity, dtype=jnp.int32)[None, :]).astype(
        jnp.bfloat16
    )


def local(
    tokens,
    state,
    norm_gain,
    w_query,
    w_forget,
    w_input,
    w_outgate,
    forget_floor,
    head_gain,
    w_out,
    ffn_gain,
    routes,
    route_weights,
    expert_gate,
    expert_up,
    expert_down,
    dense_gate,
    dense_up,
    dense_down,
    dense_mix,
):
    seqs, width = tokens.shape
    local_heads = state.shape[1]
    key_size = state.shape[2]
    value_size = state.shape[3]
    resid_in = tokens.astype(jnp.float32)
    normed = rms_norm(resid_in, norm_gain).astype(jnp.bfloat16)
    zq = jnp.dot(normed, w_query, preferred_element_type=jnp.float32)
    zf = jnp.dot(normed, w_forget, preferred_element_type=jnp.float32)
    zi = jnp.dot(normed, w_input, preferred_element_type=jnp.float32)
    zg = jnp.dot(normed, w_outgate, preferred_element_type=jnp.float32)
    logf = jnp.logaddexp(jax.nn.log_sigmoid(zf), jnp.log(forget_floor) + jax.nn.log_sigmoid(-zf))
    logf = logf.reshape(seqs, local_heads, key_size)
    query = jax.nn.silu(zq).reshape(seqs, local_heads, key_size)
    keep = jnp.exp(logf)
    write = -jnp.expm1(logf)
    values = zi.reshape(seqs, local_heads, value_size)
    new_state = keep[..., None] * state + write[..., None] * values[:, :, None, :]
    read = jnp.einsum("thk,thkv->thv", query, new_state, precision=lax.Precision.HIGHEST)
    read = rms_norm(read, head_gain).reshape(seqs, local_heads * value_size)
    headout = (read * jax.nn.silu(zg)).astype(jnp.bfloat16)
    block_term = jnp.dot(headout, w_out, preferred_element_type=jnp.float32)
    block_term = block_term.astype(jnp.bfloat16).astype(jnp.float32)
    mixout = lax.psum(block_term.astype(jnp.bfloat16), "tp").astype(jnp.float32)
    resid = resid_in + mixout
    ffn_in = rms_norm(resid, ffn_gain).astype(jnp.bfloat16)
    piece = lax.all_gather(ffn_in, "ep", axis=0, tiled=True)
    dgate = jnp.dot(piece, dense_gate, preferred_element_type=jnp.float32)
    dupper = jnp.dot(piece, dense_up, preferred_element_type=jnp.float32)
    dense_hidden = (jax.nn.silu(dgate) * dupper).astype(jnp.bfloat16)
    rows = dense_hidden
    summed = lax.psum_scatter(
        jnp.dot(rows, dense_down, preferred_element_type=jnp.float32).astype(jnp.bfloat16),
        "ep",
        scatter_dimension=0,
        tiled=True,
    )
    dense = summed.astype(jnp.float32)
    experts = lax.axis_size("ep") * expert_gate.shape[0]
    top = routes.shape[1]
    capacity = 2 * seqs * top // experts
    table = make_table(routes, experts, capacity)
    repeated = jnp.repeat(ffn_in, top, axis=0)
    sent = jnp.dot(table.T, repeated, preferred_element_type=jnp.float32).astype(jnp.bfloat16)
    sent = sent.reshape(experts, capacity, width)
    arrived = lax.all_to_all(sent, "ep", split_axis=0, concat_axis=0, tiled=True)
    sources, items, _ = arrived.shape
    rows = arrived.reshape(sources * items, width)
    gate = jnp.dot(rows, expert_gate[0], preferred_element_type=jnp.float32)
    upper = jnp.dot(rows, expert_up[0], preferred_element_type=jnp.float32)
    hidden = (jax.nn.silu(gate) * upper).astype(jnp.bfloat16)
    part = jnp.dot(hidden, expert_down[0], preferred_element_type=jnp.float32)
    part = part.astype(jnp.bfloat16).astype(jnp.float32)
    summed_parts = lax.psum(part.astype(jnp.bfloat16), "tp")
    results = summed_parts.reshape(sources, items, width)
    back = lax.all_to_all(results, "ep", split_axis=0, concat_axis=0, tiled=True)
    picked = jnp.dot(
        table, back.reshape(experts * capacity, width), preferred_element_type=jnp.float32
    )
    weighted = picked * route_weights.reshape(seqs * top)[:, None]
    moe = jnp.sum(weighted.reshape(seqs, top, width), axis=1)
    mixed = (resid + moe + jax.nn.sigmoid(dense_mix) * dense).astype(jnp.bfloat16)
    return (mixed, new_state)


def solution(mesh):
    in_specs = (
        P("ep", None),
        P("ep", "tp", None, None),
        P(),
        P(None, "tp"),
        P(None, "tp"),
        P(None, "tp"),
        P(None, "tp"),
        P("tp"),
        P(),
        P("tp", None),
        P(),
        P("ep", None),
        P("ep", None),
        P("ep", None, "tp"),
        P("ep", None, "tp"),
        P("ep", "tp", None),
        P(None, "ep"),
        P(None, "ep"),
        P("ep", None),
        P(),
    )
    out_specs = (P("ep", None), P("ep", "tp", None, None))
    return jax.shard_map(local, mesh=mesh, in_specs=in_specs, out_specs=out_specs, check_vma=False)
```

profile of v0, /device:TPU:0, one launch (start us, length us, event | category | flops | bytes accessed | tf_op | source)
XLA Modules:
  0.0 235.8 jit_solution(614285579938243527)
XLA Ops:
  7.3 1.2 fusion.20
  8.5 2.2 divide_multiply_fusion
  10.7 2.2 fusion.38
  13.0 2.3 fusion.35
  15.3 8.2 %multiply_add_fusion = f32[32,4,128,128]{3,2,1,0:T(8,128)S(1)} fusion(f32[32,4,128,128]{3,2,1,0:T(8,128)} %param.21, f32[32,4,128]{2,1,0:T(4,128)S(1)} %mul.144, f32[32,4,128]{2,1,0:T(4,128)S(1)} %neg.60, f32[32,4,128]{2,1,0:T(4,128)S(1)} %exp.44), kind=kLoop, calls=%fused_computation | loop fusion | flops 6291456 | bytes 16973824 | tf_op jit(solution)/shard_map/add | solution.py:62
  23.6 7.3 %fusion.50 = f32[32,4,1,128]{3,2,1,0:T(1,128)S(1)} fusion(f32[32,4,128,1]{2,3,1,0:T(1,128)S(1)} %bitcast.52, f32[32,4,128,128]{3,2,1,0:T(8,128)S(1)} %multiply_add_fusion), kind=kOutput, calls=%fused_computation.59 | convolution fusion | flops 25165824 | bytes 8519680 | tf_op jit(solution)/shard_map/thk,thkv->thv/dot_general | solution.py:63
  31.1 3.8 %convolution_convert_fusion.2 = bf16[32,2048]{1,0:T(8,128)(2,1)} fusion(bf16[512,2048]{1,0:T(8,128)(2,1)} %param.29, f32[4,8,4,128]{3,2,1,0:T(4,128)S(1)} %bitcast.53, bf16[2048,512]{1,0:T(8,128)(2,1)} %param.26, bf16[32,2048]{1,0:T(8,128)(2,1)S(1)} %copy-done.2, f32[2048]{0:T(1024)S(1)} %copy-done.4, f32[32]{0:T(128)S(1)} %add_rsqrt_fusion.2), kind=kOutput, calls=%fused_computation.13 | convolution fusion | flops 134643712 | bytes 4530304 | tf_op jit(solution)/shard_map/dot_general | solution.py:66
  35.5 34.1 %all-reduce.3.cloned.1.call-done = bf16[32,2048]{1,0:T(8,128)(2,1)} async-done(((bf16[32,2048]{1,0:T(8,128)(2,1)}), bf16[32,2048]{1,0:T(8,128)(2,1)}) %all-reduce.3.cloned.1.call-update) | async-done | bytes 131088 | tf_op jit(solution)/shard_map/psum | solution.py:68
  72.6 2.1 convolution_convert_fusion.1
  74.8 5.5 %all-to-all-start = ((bf16[8,16,2048]{2,1,0:T(8,128)(2,1)}), bf16[8,16,2048]{2,1,0:T(8,128)(2,1)S(1)}, u32[]{:S(2)}, u32[]{:S(2)}) async-start(bf16[8,16,2048]{2,1,0:T(8,128)(2,1)} %bitcast.3), calls=%async_computation | async-start | bytes 1048576 | tf_op jit(solution)/shard_map/all_to_all | solution.py:90
  81.3 12.4 %all-to-all-done = bf16[8,16,2048]{2,1,0:T(8,128)(2,1)S(1)} async-done(((bf16[8,16,2048]{2,1,0:T(8,128)(2,1)}), bf16[8,16,2048]{2,1,0:T(8,128)(2,1)S(1)}, u32[]{:S(2)}, u32[]{:S(2)}) %all-to-all-start) | async-done | bytes 524320 | tf_op jit(solution)/shard_map/all_to_all | solution.py:90
  93.7 4.5 %fusion.4 = f32[128,1408]{1,0:T(8,128)} fusion(bf16[128,2048]{1,0:T(8,128)(2,1)S(1)} %bitcast.47, bf16[1,2048,1408]{2,1,0:T(8,128)(2,1)} %param.33), kind=kOutput, calls=%fused_computation.5 | convolution fusion | flops 738197504 | bytes 7012352 | tf_op jit(solution)/shard_map/dot_general | solution.py:93
  98.2 7.3 %fusion.12 = bf16[128,2048]{1,0:T(8,128)(2,1)} fusion(bf16[1,1408,2048]{2,1,0:T(8,128)(2,1)} %param.35, bf16[128,2048]{1,0:T(8,128)(2,1)S(1)} %bitcast.48, bf16[1,2048,1408]{2,1,0:T(8,128)(2,1)} %param.34, f32[128,1408]{1,0:T(8,128)} %fusion.4), kind=kOutput, calls=%fused_computation.11 | convolution fusion | flops 1477738496 | bytes 13303808 | tf_op jit(solution)/shard_map/dot_general | solution.py:96
  105.6 19.0 %all-gather.2.cloned.1.call-done = bf16[256,2048]{1,0:T(8,128)(2,1)} async-done(((bf16[32,2048]{1,0:T(8,128)(2,1)}), bf16[256,2048]{1,0:T(8,128)(2,1)}) %all-gather.2.cloned.1.call-update) | async-done | bytes 1048592 | tf_op jit(solution)/shard_map/all_gather | solution.py:71
  124.6 4.0 %fusion.51 = f32[256,704]{0,1:T(8,128)} fusion(bf16[256,2048]{1,0:T(8,128)(2,1)} %all-gather.2.cloned.1.call-done, bf16[2048,704]{0,1:T(8,128)(2,1)} %param.36), kind=kOutput, calls=%fused_computation.60 | convolution fusion | flops 738197504 | bytes 4653056 | tf_op jit(solution)/shard_map/dot_general | solution.py:72
  128.6 6.6 %convolution_convert_fusion = bf16[256,2048]{1,0:T(8,128)(2,1)} fusion(bf16[704,2048]{1,0:T(8,128)(2,1)S(1)} %copy-done, bf16[256,2048]{1,0:T(8,128)(2,1)} %all-gather.2.cloned.1.call-done, bf16[2048,704]{0,1:T(8,128)(2,1)} %param.37, f32[256,704]{0,1:T(8,128)} %fusion.51), kind=kOutput, calls=%fused_computation.7 | convolution fusion | flops 1478000640 | bytes 8585216 | tf_op jit(solution)/shard_map/dot_general | solution.py:77
  135.2 23.9 %all-reduce.5.cloned.1.call-done = bf16[8,16,2048]{2,1,0:T(8,128)(2,1)} async-done(((bf16[8,16,2048]{2,1,0:T(8,128)(2,1)}), bf16[8,16,2048]{2,1,0:T(8,128)(2,1)}) %all-reduce.5.cloned.1.call-update) | async-done | bytes 524304 | tf_op jit(solution)/shard_map/psum | solution.py:98
  159.1 5.5 %all-to-all-start.1 = ((bf16[8,16,2048]{2,1,0:T(8,128)(2,1)}), bf16[8,16,2048]{2,1,0:T(8,128)(2,1)S(1)}, u32[]{:S(2)}, u32[]{:S(2)}) async-start(bf16[8,16,2048]{2,1,0:T(8,128)(2,1)} %all-reduce.5.cloned.1.call-done), calls=%async_computation.1 | async-start | bytes 1048576 | tf_op jit(solution)/shard_map/all_to_all | solution.py:100
  166.7 15.4 %all-to-all-done.1 = bf16[8,16,2048]{2,1,0:T(8,128)(2,1)S(1)} async-done(((bf16[8,16,2048]{2,1,0:T(8,128)(2,1)}), bf16[8,16,2048]{2,1,0:T(8,128)(2,1)S(1)}, u32[]{:S(2)}, u32[]{:S(2)}) %all-to-all-start.1) | async-done | bytes 524320 | tf_op jit(solution)/shard_map/all_to_all | solution.py:100
  182.1 1.8 convolution_multiply_fusion
  183.8 1.4 reshape.94
  185.2 1.3 reduce_sum.49
  186.5 40.9 %reduce-scatter.2.cloned.1.call-done = bf16[32,2048]{1,0:T(8,128)(2,1)} async-done(((bf16[256,2048]{1,0:T(8,128)(2,1)}), bf16[32,2048]{1,0:T(8,128)(2,1)}) %reduce-scatter.2.cloned.1.call-update) | async-done | bytes 131088 | tf_op jit(solution)/shard_map/reduce_scatter | solution.py:76
  227.5 1.8 add_convert_fusion
  (51 shorter events, 7.1 us)
Async XLA Ops:
  7.2 121.4 %copy-start = (bf16[704,2048]{1,0:T(8,128)(2,1)S(1)}, bf16[704,2048]{1,0:T(8,128)(2,1)}, u32[]{:S(2)}) copy-start(bf16[704,2048]{1,0:T(8,128)(2,1)} %param.38) | copy-start | bytes 8650756
  7.2 5.8 %copy-start.2 = (bf16[32,2048]{1,0:T(8,128)(2,1)S(1)}, bf16[32,2048]{1,0:T(8,128)(2,1)}, u32[]{:S(2)}) copy-start(bf16[32,2048]{1,0:T(8,128)(2,1)} %param.20) | copy-start | bytes 393220
  7.2 5.8 %copy-start.4 = (f32[2048]{0:T(1024)S(1)}, f32[2048]{0:T(1024)}, u32[]{:S(2)}) copy-start(f32[2048]{0:T(1024)} %param.22) | copy-start | bytes 24580
  7.2 5.7 %copy-start.7 = (f32[512]{0:T(512)S(1)}, f32[512]{0:T(512)}, u32[]{:S(2)}) copy-start(f32[512]{0:T(512)} %param.27) | copy-start | bytes 6148
  7.2 62.4 %all-reduce.3.cloned.1.call-start = ((), (), s32[]{:S(2)}) async-start(), calls=%async_computation.3 | async-start | bytes 262144 | tf_op jit(solution)/shard_map/psum | solution.py:68
  23.5 7.3 %copy-start.1 = (f32[32,4,128,128]{3,2,1,0:T(8,128)}, f32[32,4,128,128]{3,2,1,0:T(8,128)S(1)}, u32[]{:S(2)}) copy-start(f32[32,4,128,128]{3,2,1,0:T(8,128)S(1)} %multiply_add_fusion) | copy-start | bytes 25165828
  23.6 7.4 %copy-start.9 = (f32[128]{0:T(128)S(1)}, f32[128]{0:T(128)}, u32[]{:S(2)}) copy-start(f32[128]{0:T(128)} %param.28) | copy-start | bytes 1540
  30.8 4.1 %copy-start.8 = (s32[32,2]{0,1:T(2,128)S(1)}, s32[32,2]{0,1:T(2,128)}, u32[]{:S(2)}) copy-start(s32[32,2]{0,1:T(2,128)} %param.31) | copy-start | bytes 772
  30.8 39.9 %copy-start.5 = (f32[2048]{0:T(1024)S(1)}, f32[2048]{0:T(1024)}, u32[]{:S(2)}) copy-start(f32[2048]{0:T(1024)} %param.30) | copy-start | bytes 24580
  35.5 39.3 %copy-start.6 = (s32[64]{0:T(128)}, s32[64]{0:T(128)S(1)}, u32[]{:S(2)}) copy-start(s32[64]{0:T(128)S(1)} %multiply_add_fusion.1) | copy-start | bytes 772
  71.7 3.1 %copy-start.3 = (bf16[32,2048]{1,0:T(8,128)(2,1)}, bf16[32,2048]{1,0:T(8,128)(2,1)S(1)}, u32[]{:S(2)}) copy-start(bf16[32,2048]{1,0:T(8,128)(2,1)S(1)} %multiply_convert_fusion) | copy-start | bytes 393220
  74.8 18.9 %all-to-all-start = ((bf16[8,16,2048]{2,1,0:T(8,128)(2,1)}), bf16[8,16,2048]{2,1,0:T(8,128)(2,1)S(1)}, u32[]{:S(2)}, u32[]{:S(2)}) async-start(bf16[8,16,2048]{2,1,0:T(8,128)(2,1)} %bitcast.3), calls=%async_computation | async-start | bytes 1048576 | tf_op jit(solution)/shard_map/all_to_all | solution.py:90
  80.3 44.3 %all-gather.2.cloned.1.call-start = ((), (), s32[]{:S(2)}) async-start(), calls=%async_computation.5 | async-start | bytes 1179648 | tf_op jit(solution)/shard_map/all_gather | solution.py:71
  81.1 78.1 %all-reduce.5.cloned.1.call-start = ((), (), s32[]{:S(2)}) async-start(), calls=%async_computation.4 | async-start | bytes 1048576 | tf_op jit(solution)/shard_map/psum | solution.py:98
  105.5 121.9 %reduce-scatter.2.cloned.1.call-start = ((), (), s32[]{:S(2)}) async-start(), calls=%async_computation.6 | async-start | bytes 1179648 | tf_op jit(solution)/shard_map/reduce_scatter | solution.py:76
  159.1 23.0 %all-to-all-start.1 = ((bf16[8,16,2048]{2,1,0:T(8,128)(2,1)}), bf16[8,16,2048]{2,1,0:T(8,128)(2,1)S(1)}, u32[]{:S(2)}, u32[]{:S(2)}) async-start(bf16[8,16,2048]{2,1,0:T(8,128)(2,1)} %all-reduce.5.cloned.1.call-done), calls=%async_computation.1 | async-start | bytes 1048576 | tf_op jit(solution)/shard_map/all_to_all | solution.py:100
Sparse Core Ops, SparseCore 0:
  35.1 34.4 all-reduce.2
  83.8 40.7 all-gather.1
  127.0 32.1 all-reduce.4
  162.4 65.0 reduce-scatter.1
where the time goes:
time: 237 us; the launch traced here: 236 us
  waiting for transfers between devices  147 us (62%)
  matrix products  44 us (19%)
  other arithmetic  15.9 us (7%)
  between operations  14 us (6%)
  starting transfers between devices  11.4 us (5%)
  local copies, waits for them, and re-layouts  4.03 us (2%)
    reduce_scatter x1, waiting for transfers between devices, local(): lax.psum_scatter(jnp.dot(rows, dense_down, preferred_element_type=jnp.flo...  40.9 us
    psum x1, waiting for transfers between devices, local(): mixout = lax.psum(block_term.astype(jnp.bfloat16), 'tp').astype(jnp.float32)  34.1 us
    psum x1, waiting for transfers between devices, local(): summed_parts = lax.psum(part.astype(jnp.bfloat16), 'tp')  23.9 us
    all_gather x1, waiting for transfers between devices, local(): piece = lax.all_gather(ffn_in, 'ep', axis=0, tiled=True)  19 us
    all_to_all x1, waiting for transfers between devices, local(): lax.all_to_all(results, 'ep', split_axis=0, concat_axis=0, tiled=True)  15.4 us
    all_to_all x1, waiting for transfers between devices, local(): lax.all_to_all(sent, 'ep', split_axis=0, concat_axis=0, tiled=True)  12.4 us
    add x1, other arithmetic, local(): keep[..., None] * state + write[..., None] * values[:, :, None, :]  8.22 us
    dot_general x1, matrix products, local(): part = jnp.dot(hidden, expert_down[0], preferred_element_type=jnp.float32)  7.29 us
  transfers between devices with their start and end apart: 6, of which 6 were waited for; matrix products, arithmetic and copies ran while one was open for 12% of the time, Pallas kernels for 0%

commit v1 on v0

--- a/solution.py
+++ b/solution.py
@@ -68,7 +68,9 @@
     mixout = lax.psum(block_term.astype(jnp.bfloat16), "tp").astype(jnp.float32)
     resid = resid_in + mixout
     ffn_in = rms_norm(resid, ffn_gain).astype(jnp.bfloat16)
-    piece = lax.all_gather(ffn_in, "ep", axis=0, tiled=True)
+    piece = jnp.concatenate(
+        lax.all_to_all(jnp.stack([ffn_in] * lax.axis_size("ep")), "ep", 0, 0), axis=0
+    )
     dgate = jnp.dot(piece, dense_gate, preferred_element_type=jnp.float32)
     dupper = jnp.dot(piece, dense_up, preferred_element_type=jnp.float32)
     dense_hidden = (jax.nn.silu(dgate) * dupper).astype(jnp.bfloat16)

time: 237 us -> 222 us (0.937)
  waiting for transfers between devices: 147 us -> 114 us
  blocking collectives: 0 us -> 18.7 us
    all_gather x1 -> x0, waiting for transfers between devices: 19 us -> none  [local(): piece = lax.all_gather(ffn_in, 'ep', axis=0, tiled=True)]
    all_to_all x0 -> x1, blocking collectives: none -> 18.7 us  [local(): lax.all_to_all(sent, 'ep', split_axis=0, concat_axis=0, tiled=True)]
    psum x1, waiting for transfers between devices: 23.9 us -> 10.4 us  [local(): summed_parts = lax.psum(part.astype(jnp.bfloat16), 'tp')]
  transfers between devices with their start and end apart: 6 -> 5, of which waited for: 6 -> 5; matrix products, arithmetic and copies ran while one was open for 12% -> 13% of each run, Pallas kernels for 0% -> 0%
where the time goes in v1:
time: 222 us; the launch traced here: 221 us
  waiting for transfers between devices  114 us (51%)
  matrix products  42.2 us (19%)
  blocking collectives  18.7 us (8%)
  other arithmetic  15.9 us (7%)
  between operations  14 us (6%)
  starting transfers between devices  10.1 us (5%)
  local copies, waits for them, and re-layouts  5.99 us (3%)
    reduce_scatter x1, waiting for transfers between devices, local(): lax.psum_scatter(jnp.dot(rows, dense_down, preferred_element_type=jnp.flo...  41.4 us
    psum x1, waiting for transfers between devices, local(): mixout = lax.psum(block_term.astype(jnp.bfloat16), 'tp').astype(jnp.float32)  34.1 us
    all_to_all x1, blocking collectives, local(): lax.all_to_all(sent, 'ep', split_axis=0, concat_axis=0, tiled=True)  18.7 us
    all_to_all x1, waiting for transfers between devices, local(): lax.all_to_all(results, 'ep', split_axis=0, concat_axis=0, tiled=True)  15.3 us
    all_to_all x1, waiting for transfers between devices, local(): lax.all_to_all(jnp.stack([ffn_in] * lax.axis_size('ep')), 'ep', 0, 0)  13 us
    psum x1, waiting for transfers between devices, local(): summed_parts = lax.psum(part.astype(jnp.bfloat16), 'tp')  10.4 us
    add x1, other arithmetic, local(): keep[..., None] * state + write[..., None] * values[:, :, None, :]  8.22 us
    dot_general x1, matrix products, local(): part = jnp.dot(hidden, expert_down[0], preferred_element_type=jnp.float32)  7.26 us
  transfers between devices with their start and end apart: 5, of which 5 were waited for; matrix products, arithmetic and copies ran while one was open for 13% of the time, Pallas kernels for 0%

profile of v1, /device:TPU:0, one launch (start us, length us, event | category | flops | bytes accessed | tf_op | source)
XLA Modules:
  0.0 221.1 jit_solution(12960436218366852924)
XLA Ops:
  7.3 1.2 fusion.20
  8.5 2.2 %divide_multiply_fusion = f32[32,512]{1,0:T(8,128)S(1)} fusion(bf16[2048,512]{1,0:T(8,128)(2,1)} %param.23, bf16[32,2048]{1,0:T(8,128)(2,1)} %param.20, f32[2048]{0:T(1024)} %param.22, f32[32]{0:T(128)S(1)} %add_rsqrt_fusion.2), kind=kOutput, calls=%fused_computation.38 | convolution fusion | flops 67436544 | bytes 2302080 | tf_op jit(solution)/shard_map/dot_general | solution.py:52
  10.7 2.2 fusion.38
  13.0 2.3 %fusion.35 = (f32[32,512]{1,0:T(8,128)S(1)}, f32[32,512]{1,0:T(8,128)S(1)}) fusion(f32[512]{0:T(512)S(1)} %log.3, bf16[2048,512]{1,0:T(8,128)(2,1)} %param.24, bf16[32,2048]{1,0:T(8,128)(2,1)S(1)} %copy-done.2, f32[2048]{0:T(1024)S(1)} %copy-done.4, f32[32]{0:T(128)S(1)} %add_rsqrt_fusion.2), kind=kOutput, calls=%fused_computation.54 | convolution fusion | flops 67780608 | bytes 2369664 | tf_op jit(solution)/shard_map/dot_general | solution.py:53
  15.3 8.2 %multiply_add_fusion = f32[32,4,128,128]{3,2,1,0:T(8,128)S(1)} fusion(f32[32,4,128,128]{3,2,1,0:T(8,128)} %param.21, f32[32,4,128]{2,1,0:T(4,128)S(1)} %mul.144, f32[32,4,128]{2,1,0:T(4,128)S(1)} %neg.60, f32[32,4,128]{2,1,0:T(4,128)S(1)} %exp.44), kind=kLoop, calls=%fused_computation | loop fusion | flops 6291456 | bytes 16973824 | tf_op jit(solution)/shard_map/add | solution.py:62
  23.6 7.3 %fusion.50 = f32[32,4,1,128]{3,2,1,0:T(1,128)S(1)} fusion(f32[32,4,128,1]{2,3,1,0:T(1,128)S(1)} %bitcast.54, f32[32,4,128,128]{3,2,1,0:T(8,128)S(1)} %multiply_add_fusion), kind=kOutput, calls=%fused_computation.59 | convolution fusion | flops 25165824 | bytes 8519680 | tf_op jit(solution)/shard_map/thk,thkv->thv/dot_general | solution.py:63
  31.1 3.8 %convolution_convert_fusion.2 = bf16[32,2048]{1,0:T(8,128)(2,1)} fusion(bf16[512,2048]{1,0:T(8,128)(2,1)} %param.29, f32[4,8,4,128]{3,2,1,0:T(4,128)S(1)} %bitcast.55, bf16[2048,512]{1,0:T(8,128)(2,1)} %param.26, bf16[32,2048]{1,0:T(8,128)(2,1)S(1)} %copy-done.2, f32[2048]{0:T(1024)S(1)} %copy-done.4, f32[32]{0:T(128)S(1)} %add_rsqrt_fusion.2), kind=kOutput, calls=%fused_computation.13 | convolution fusion | flops 134643712 | bytes 4530304 | tf_op jit(solution)/shard_map/dot_general | solution.py:66
  35.5 34.1 %all-reduce.3.cloned.1.call-done = bf16[32,2048]{1,0:T(8,128)(2,1)} async-done(((bf16[32,2048]{1,0:T(8,128)(2,1)}), bf16[32,2048]{1,0:T(8,128)(2,1)}) %all-reduce.3.cloned.1.call-update) | async-done | bytes 131088 | tf_op jit(solution)/shard_map/psum | solution.py:68
  73.0 18.7 %all_to_all.15 = bf16[8,16,2048]{2,1,0:T(8,128)(2,1)S(1)} all-to-all(bf16[8,16,2048]{2,1,0:T(8,128)(2,1)S(1)} %bitcast.48), channel_id=1, replica_groups=mesh['ep'=8,'tp'=4] {'ep'}, dimensions={0} | all-to-all | bytes 1048576 | tf_op jit(solution)/shard_map/all_to_all | solution.py:92
  91.7 2.0 stack.2
  93.8 4.2 %all-to-all-start.2 = ((bf16[8,32,2048]{2,1,0:T(8,128)(2,1)}), bf16[8,32,2048]{2,1,0:T(8,128)(2,1)}, u32[]{:S(2)}, u32[]{:S(2)}) async-start(bf16[8,32,2048]{2,1,0:T(8,128)(2,1)} %stack.2), calls=%async_computation.2 | async-start | bytes 2097152 | tf_op jit(solution)/shard_map/all_to_all | solution.py:72
  98.2 4.5 %fusion.4 = f32[128,1408]{1,0:T(8,128)} fusion(bf16[128,2048]{1,0:T(8,128)(2,1)S(1)} %bitcast.49, bf16[1,2048,1408]{2,1,0:T(8,128)(2,1)} %param.33), kind=kOutput, calls=%fused_computation.5 | convolution fusion | flops 738197504 | bytes 7012352 | tf_op jit(solution)/shard_map/dot_general | solution.py:95
  102.7 7.3 %fusion.12 = bf16[128,2048]{1,0:T(8,128)(2,1)} fusion(bf16[1,1408,2048]{2,1,0:T(8,128)(2,1)} %param.35, bf16[128,2048]{1,0:T(8,128)(2,1)S(1)} %bitcast.50, bf16[1,2048,1408]{2,1,0:T(8,128)(2,1)} %param.34, f32[128,1408]{1,0:T(8,128)} %fusion.4), kind=kOutput, calls=%fused_computation.11 | convolution fusion | flops 1477738496 | bytes 13303808 | tf_op jit(solution)/shard_map/dot_general | solution.py:98
  110.1 13.0 %all-to-all-done.2 = bf16[8,32,2048]{2,1,0:T(8,128)(2,1)} async-done(((bf16[8,32,2048]{2,1,0:T(8,128)(2,1)}), bf16[8,32,2048]{2,1,0:T(8,128)(2,1)}, u32[]{:S(2)}, u32[]{:S(2)}) %all-to-all-start.2) | async-done | bytes 1048608 | tf_op jit(solution)/shard_map/all_to_all | solution.py:72
  123.1 4.0 %fusion.51 = f32[256,704]{0,1:T(8,128)} fusion(bf16[256,2048]{1,0:T(8,128)(2,1)} %bitcast.10, bf16[2048,704]{0,1:T(8,128)(2,1)} %param.36), kind=kOutput, calls=%fused_computation.60 | convolution fusion | flops 738197504 | bytes 4653056 | tf_op jit(solution)/shard_map/dot_general | solution.py:74
  127.0 6.6 %convolution_convert_fusion = bf16[256,2048]{1,0:T(8,128)(2,1)} fusion(bf16[704,2048]{1,0:T(8,128)(2,1)S(1)} %copy-done, bf16[256,2048]{1,0:T(8,128)(2,1)} %bitcast.10, bf16[2048,704]{0,1:T(8,128)(2,1)} %param.37, f32[256,704]{0,1:T(8,128)} %fusion.51), kind=kOutput, calls=%fused_computation.7 | convolution fusion | flops 1478000640 | bytes 8585216 | tf_op jit(solution)/shard_map/dot_general | solution.py:79
  133.6 10.4 %all-reduce.5.cloned.1.call-done = bf16[8,16,2048]{2,1,0:T(8,128)(2,1)} async-done(((bf16[8,16,2048]{2,1,0:T(8,128)(2,1)}), bf16[8,16,2048]{2,1,0:T(8,128)(2,1)}) %all-reduce.5.cloned.1.call-update) | async-done | bytes 524304 | tf_op jit(solution)/shard_map/psum | solution.py:100
  144.0 5.5 %all-to-all-start.1 = ((bf16[8,16,2048]{2,1,0:T(8,128)(2,1)}), bf16[8,16,2048]{2,1,0:T(8,128)(2,1)S(1)}, u32[]{:S(2)}, u32[]{:S(2)}) async-start(bf16[8,16,2048]{2,1,0:T(8,128)(2,1)} %all-reduce.5.cloned.1.call-done), calls=%async_computation.1 | async-start | bytes 1048576 | tf_op jit(solution)/shard_map/all_to_all | solution.py:102
  151.6 15.3 %all-to-all-done.1 = bf16[8,16,2048]{2,1,0:T(8,128)(2,1)S(1)} async-done(((bf16[8,16,2048]{2,1,0:T(8,128)(2,1)}), bf16[8,16,2048]{2,1,0:T(8,128)(2,1)S(1)}, u32[]{:S(2)}, u32[]{:S(2)}) %all-to-all-start.1) | async-done | bytes 524320 | tf_op jit(solution)/shard_map/all_to_all | solution.py:102
  166.9 1.8 convolution_multiply_fusion
  168.7 1.4 reshape.99
  170.0 1.4 reduce_sum.49
  171.4 41.4 %reduce-scatter.2.cloned.1.call-done = bf16[32,2048]{1,0:T(8,128)(2,1)} async-done(((bf16[256,2048]{1,0:T(8,128)(2,1)}), bf16[32,2048]{1,0:T(8,128)(2,1)}) %reduce-scatter.2.cloned.1.call-update) | async-done | bytes 131088 | tf_op jit(solution)/shard_map/reduce_scatter | solution.py:78
  212.8 1.8 add_convert_fusion
  (50 shorter events, 6.7 us)
Async XLA Ops:
  7.2 119.9 %copy-start = (bf16[704,2048]{1,0:T(8,128)(2,1)S(1)}, bf16[704,2048]{1,0:T(8,128)(2,1)}, u32[]{:S(2)}) copy-start(bf16[704,2048]{1,0:T(8,128)(2,1)} %param.38) | copy-start | bytes 8650756
  7.2 5.8 %copy-start.2 = (bf16[32,2048]{1,0:T(8,128)(2,1)S(1)}, bf16[32,2048]{1,0:T(8,128)(2,1)}, u32[]{:S(2)}) copy-start(bf16[32,2048]{1,0:T(8,128)(2,1)} %param.20) | copy-start | bytes 393220
  7.2 5.8 %copy-start.4 = (f32[2048]{0:T(1024)S(1)}, f32[2048]{0:T(1024)}, u32[]{:S(2)}) copy-start(f32[2048]{0:T(1024)} %param.22) | copy-start | bytes 24580
  7.2 5.7 %copy-start.7 = (f32[512]{0:T(512)S(1)}, f32[512]{0:T(512)}, u32[]{:S(2)}) copy-start(f32[512]{0:T(512)} %param.27) | copy-start | bytes 6148
  7.2 62.4 %all-reduce.3.cloned.1.call-start = ((), (), s32[]{:S(2)}) async-start(), calls=%async_computation.4 | async-start | bytes 262144 | tf_op jit(solution)/shard_map/psum | solution.py:68
  23.5 7.3 %copy-start.1 = (f32[32,4,128,128]{3,2,1,0:T(8,128)}, f32[32,4,128,128]{3,2,1,0:T(8,128)S(1)}, u32[]{:S(2)}) copy-start(f32[32,4,128,128]{3,2,1,0:T(8,128)S(1)} %multiply_add_fusion) | copy-start | bytes 25165828
  23.6 7.4 %copy-start.9 = (f32[128]{0:T(128)S(1)}, f32[128]{0:T(128)}, u32[]{:S(2)}) copy-start(f32[128]{0:T(128)} %param.28) | copy-start | bytes 1540
  30.8 4.1 %copy-start.8 = (s32[32,2]{0,1:T(2,128)S(1)}, s32[32,2]{0,1:T(2,128)}, u32[]{:S(2)}) copy-start(s32[32,2]{0,1:T(2,128)} %param.31) | copy-start | bytes 772
  30.8 39.9 %copy-start.5 = (f32[2048]{0:T(1024)S(1)}, f32[2048]{0:T(1024)}, u32[]{:S(2)}) copy-start(f32[2048]{0:T(1024)} %param.30) | copy-start | bytes 24580
  35.5 58.2 %copy-start.6 = (s32[64]{0:T(128)}, s32[64]{0:T(128)S(1)}, u32[]{:S(2)}) copy-start(s32[64]{0:T(128)S(1)} %multiply_add_fusion.1) | copy-start | bytes 772
  71.7 0.7 copy-start.3
  93.8 29.3 %all-to-all-start.2 = ((bf16[8,32,2048]{2,1,0:T(8,128)(2,1)}), bf16[8,32,2048]{2,1,0:T(8,128)(2,1)}, u32[]{:S(2)}, u32[]{:S(2)}) async-start(bf16[8,32,2048]{2,1,0:T(8,128)(2,1)} %stack.2), calls=%async_computation.2 | async-start | bytes 2097152 | tf_op jit(solution)/shard_map/all_to_all | solution.py:72
  98.0 46.0 %all-reduce.5.cloned.1.call-start = ((), (), s32[]{:S(2)}) async-start(), calls=%async_computation.5 | async-start | bytes 1048576 | tf_op jit(solution)/shard_map/psum | solution.py:100
  110.0 102.8 %reduce-scatter.2.cloned.1.call-start = ((), (), s32[]{:S(2)}) async-start(), calls=%async_computation.6 | async-start | bytes 1179648 | tf_op jit(solution)/shard_map/reduce_scatter | solution.py:78
  144.0 22.9 %all-to-all-start.1 = ((bf16[8,16,2048]{2,1,0:T(8,128)(2,1)}), bf16[8,16,2048]{2,1,0:T(8,128)(2,1)S(1)}, u32[]{:S(2)}, u32[]{:S(2)}) async-start(bf16[8,16,2048]{2,1,0:T(8,128)(2,1)} %all-reduce.5.cloned.1.call-done), calls=%async_computation.1 | async-start | bytes 1048576 | tf_op jit(solution)/shard_map/all_to_all | solution.py:102
Sparse Core Ops, SparseCore 0:
  35.1 34.4 all-reduce.2
  110.1 33.8 all-reduce.4
  147.4 65.3 reduce-scatter.1
